TPU v7x, 128 devices: a whole 4x4x4 slice. The times are simulated.
128 devices in a mesh: rep: 2 (over z_hi), fs: 32 (over z_lo, y, x), tp: 2 (over core).
Axes of the slice: x: 4, y: 4, z: 4 (z_hi: 2, z_lo: 2; z = z_hi * 2 + z_lo), core: 2. Of those that a mesh axis runs over, the one named last changes fastest.
Arguments:
- residual: bfloat16 [32768, 2048], P(('rep', 'fs', 'tp')), may hold values from -6 to 6
- mixer_gain: float32 [2048], replicated, may hold values from 0.1 to 1.9
- gating_proj: bfloat16 [2048, 2048], P('fs', 'tp'), may hold values from -0.125 to 0.125
- spatial_proj: bfloat16 [2048, 2048], P('fs', 'tp'), as said below
- spatial_gain: float32 [2048], replicated, may hold values from 0.1 to 1.9
- spatial_bias: float32 [2048], replicated, may hold values from -3 to 3
- spatial_mix: bfloat16 [32, 128, 128], replicated, may hold values from -0.5 to 0.5
- spatial_offset: float32 [32, 128], replicated, may hold values from 0.5 to 1.5
- mixer_out: bfloat16 [2048, 2048], P('tp', 'fs'), may hold values from -0.125 to 0.125
- channel_gain: float32 [2048], replicated, may hold values from 0.1 to 1.9
- gate_proj: bfloat16 [2048, 2816], P('fs', 'tp'), may hold values from -0.125 to 0.125
- up_proj: bfloat16 [2048, 2816], P('fs', 'tp'), may hold values from -0.125 to 0.125
- conv_taps: float32 [3, 2816], replicated, may hold values from -3.5 to 3.5
- down_proj: bfloat16 [2816, 2048], P('tp', 'fs'), may hold values from -0.109375 to 0.109375
Outputs:
- layer_out: bfloat16 [32768, 2048], P(('rep', 'fs', 'tp'))
Inputs may be any that keep to these rules, and one draw needn't show every extreme that they name: `spatial_proj`: entries are bounded in magnitude by 56 / sqrt(2048).
All inputs are finite; a program needn't handle non-finite values.
Results may differ from a plain program's by a relative error of at most 0.015.
Values may be sent and summed in bfloat16 or wider, within the bound.
No kernel may reach another device: no remote copies, remote signals or barrier semaphores. Data moves between devices by JAX's collectives and lax.ppermute only.
A program may use at most 128 MiB of HBM per device.

v0:
```python
import jax
import jax.numpy as jnp
from jax import lax
from jax.sharding import Mesh
from jax.sharding import PartitionSpec as P

HEAD = 64
GROUP = 2048
BLOCK = 128
SEGMENT = 64
KCONV = 3
SEQ_LEN = 256
FS = ("fs_0", "fs_1", "fs_2")
REP_FS_TP = ("rep", "fs_0", "fs_1", "fs_2", "tp")


def in_order(pieces, dim):
    pieces = jnp.moveaxis(pieces, 0, dim)
    lengths = pieces.shape
    return pieces.reshape(*lengths[:dim], lengths[dim] * lengths[dim + 1], *lengths[dim + 2 :])


def copy_for_each(value, axis):
    devices = lax.axis_size(axis)
    return lax.all_to_all(
        jnp.broadcast_to(value[None], (devices, *value.shape)), axis, 0, 0, tiled=True
    )


def gathered_copies(value, axis, dim):
    return in_order(copy_for_each(value, axis), dim)


def side_by_side(arrays, axis, dim, along):
    widths = [a.shape[along] for a in arrays]
    both = jnp.concatenate(arrays, axis=along)
    out = lax.all_gather(both, axis, axis=dim, tiled=True)
    return tuple(jnp.split(out, [sum(widths[:k]) for k in range(1, len(widths))], axis=along))


def of_everyone(value, axis):
    return copy_for_each(value, axis).sum(axis=0)


def in_one(arrays, axis):
    ends = [0]
    for a in arrays:
        ends.append(ends[-1] + a.size)
    running = of_everyone(jnp.concatenate([a.ravel() for a in arrays]), axis)
    return tuple((running[b:e].reshape(a.shape) for a, b, e in zip(arrays, ends, ends[1:])))


def stacked_from(value, axes, order):
    pieces = value[None]
    for k in order:
        pieces = lax.all_gather(pieces, axes[k], axis=0, tiled=True)
    block = [lax.axis_size(axes[k]) for k in reversed(order)]
    pieces = pieces.reshape(*block, *value.shape)
    turned = sorted(range(len(order)), key=lambda place: order[len(order) - 1 - place])
    return pieces.transpose(*turned, *range(len(order), pieces.ndim)).reshape(-1, *value.shape)


def gather_axes(value, axes, order, dim):
    return in_order(stacked_from(value, axes, order), dim)


def cut_along(value, dim, devices):
    before, after = (value.shape[:dim], value.shape[dim + 1 :])
    return jnp.moveaxis(value.reshape(*before, devices, -1, *after), dim, 0)


def sum_at_owner(value, axis, dim):
    pieces = cut_along(value, dim, lax.axis_size(axis))
    arrived = lax.all_to_all(pieces, axis, split_axis=0, concat_axis=0, tiled=True)
    return arrived.astype(jnp.float32).sum(axis=0)


def round_trip(value):
    return lax.optimization_barrier(value.astype(jnp.bfloat16)).astype(jnp.float32)


def rms_normed(value, gain):
    wide = value.astype(jnp.float32)
    scale = lax.rsqrt(jnp.mean(wide * wide, axis=-1, keepdims=True) + 1e-06)
    return (wide * scale * gain).astype(jnp.bfloat16)


def fold_pair(normed, pieces):
    first = jnp.dot(normed, pieces[0], preferred_element_type=jnp.float32)
    second = jnp.dot(normed, pieces[1], preferred_element_type=jnp.float32)
    return (first, second)


def on_device(
    residual,
    mixer_gain,
    gating_proj,
    spatial_proj,
    spatial_gain,
    spatial_bias,
    spatial_mix,
    spatial_offset,
    mixer_out,
    channel_gain,
    gate_proj,
    up_proj,
    conv_taps,
    down_proj,
):
    position = lax.axis_index("tp")
    rows = gathered_copies(residual, "tp", 0)
    group_rows = rows.shape[0]
    normed = rms_normed(rows, mixer_gain)
    width = gating_proj.shape[1]
    gating, spatial = fold_pair(normed, side_by_side((gating_proj, spatial_proj), FS, 0, 1))
    act_u = jax.nn.gelu(round_trip(gating))
    act_v = jax.nn.gelu(round_trip(spatial))
    total, squares = in_one((jnp.sum(act_v, axis=-1), jnp.sum(act_v * act_v, axis=-1)), "tp")
    mean = (total / GROUP)[:, None]
    var = (squares / GROUP)[:, None] - mean * mean
    gain_here = lax.dynamic_slice_in_dim(spatial_gain, position * width, width)
    bias_here = lax.dynamic_slice_in_dim(spatial_bias, position * width, width)
    vnorm = ((act_v - mean) * lax.rsqrt(var + 1e-05) * gain_here + bias_here).astype(jnp.bfloat16)
    heads_here = width // HEAD
    mix_here = lax.dynamic_slice_in_dim(spatial_mix, position * heads_here, heads_here, 0)
    offset_here = lax.dynamic_slice_in_dim(spatial_offset, position * heads_here, heads_here, 0)
    place = jnp.arange(BLOCK) // SEGMENT
    allowed = place[None, :] <= place[:, None]
    weights = jnp.where(allowed[None], mix_here, jnp.zeros_like(mix_here))
    blocks = vnorm.reshape(group_rows // BLOCK, BLOCK, heads_here, HEAD)
    mixed = jnp.einsum("hij,njhd->nihd", weights, blocks, preferred_element_type=jnp.float32)
    mixed = mixed + offset_here.T[None, :, :, None]
    gated = (act_u * mixed.reshape(group_rows, width)).astype(jnp.bfloat16)
    out_whole = gather_axes(mixer_out, FS, (0, 1, 2), 1)
    part = gated
    mixer_part = sum_at_owner(
        jnp.dot(part, out_whole, preferred_element_type=jnp.float32).astype(jnp.bfloat16), "tp", 0
    )
    middle = (residual.astype(jnp.float32) + mixer_part).astype(jnp.bfloat16)
    rows2 = gathered_copies(middle, "tp", 0)
    normed2 = rms_normed(rows2, channel_gain)
    units = gate_proj.shape[1]
    gate_whole, up_whole = side_by_side((gate_proj, up_proj), FS, 0, 1)
    gate = jnp.dot(normed2, gate_whole, preferred_element_type=jnp.float32)
    up = jnp.dot(normed2, up_whole, preferred_element_type=jnp.float32)
    gate = round_trip(gate)
    up = round_trip(up)
    taps_here = lax.dynamic_slice_in_dim(conv_taps, position * units, units, 1)
    offset = jnp.arange(group_rows) % SEQ_LEN
    conv = taps_here[KCONV - 1] * gate
    for lag in range(1, KCONV):
        shifted = jnp.concatenate([jnp.zeros((lag, units), jnp.float32), gate[:-lag]], axis=0)
        shifted = jnp.where((offset >= lag)[:, None], shifted, 0.0)
        conv = conv + taps_here[KCONV - 1 - lag] * shifted
    hidden = (jax.nn.silu(conv) * up).astype(jnp.bfloat16)
    down_whole = lax.all_gather(down_proj, FS, axis=1, tiled=True)
    part = hidden
    channel_part = sum_at_owner(
        jnp.dot(part, down_whole, preferred_element_type=jnp.float32).astype(jnp.bfloat16), "tp", 0
    )
    return (middle.astype(jnp.float32) + channel_part).astype(jnp.bfloat16)


def solution(mesh):
    split = Mesh(
        mesh.devices.reshape(mesh.shape["rep"], 2, 4, 4, mesh.shape["tp"]),
        ("rep", "fs_0", "fs_1", "fs_2", "tp"),
    )
    placed = (
        P(REP_FS_TP, None),
        P(),
        P(FS, "tp"),
        P(FS, "tp"),
        P(),
        P(),
        P(),
        P(),
        P("tp", FS),
        P(),
        P(FS, "tp"),
        P(FS, "tp"),
        P(),
        P("tp", FS),
    )
    return jax.shard_map(
        on_device, mesh=split, in_specs=placed, out_specs=P(REP_FS_TP, None), check_vma=False
    )
```

profile of v0, /device:TPU:1, one launch (start us, length us, event | category | flops | bytes accessed | tf_op | source)
XLA Modules:
  0.0 617.4 jit_solution(9370628572742280357)
XLA Ops:
  6.6 6.7 %all-gather = bf16[2048,64]{0,1:T(8,128)(2,1)S(1)} all-gather(bf16[1024,64]{0,1:T(8,128)(2,1)} %param.22), channel_id=2, replica_groups=mesh['rep'=2,'fs_0'=2,'fs_1'=4,'fs_2'=4,'tp'=2] {'fs_0'}, dimensions={0}, use_global_device_ids=true | all-gather | bytes 393216 | tf_op jit(solution)/shard_map/all_gather | solution.py:56
  13.3 0.7 copy.73
  14.1 0.0 all-gather.11.cloned.1.call-start
  14.1 24.9 %all-gather.9.cloned.1.call-done = bf16[8,1024,64]{1,2,0:T(8,128)(2,1)} async-done(((bf16[2,1024,64]{1,2,0:T(8,128)(2,1)}), bf16[8,1024,64]{1,2,0:T(8,128)(2,1)}) %all-gather.9.cloned.1.call-update) | async-done | bytes 1048592 | tf_op jit(solution)/shard_map/all_gather | solution.py:56
  39.1 0.7 pad_maximum_fusion.1
  39.8 0.0 all-gather.13.cloned.1.call-start
  39.9 0.8 pad_maximum_fusion
  40.7 0.5 all-gather.15.cloned.1.call-update
  41.3 1.6 broadcast_in_dim.32
  42.9 6.5 %all-to-all-start = ((bf16[2,256,2048]{2,1,0:T(8,128)(2,1)}), bf16[2,256,2048]{2,1,0:T(8,128)(2,1)S(1)}, u32[]{:S(2)}, u32[]{:S(2)}) async-start(bf16[2,256,2048]{2,1,0:T(8,128)(2,1)} %broadcast_in_dim.32), calls=%async_computation | async-start | bytes 4194304 | tf_op jit(solution)/shard_map/all_to_all | solution.py:25
  49.4 2.5 all-to-all-done
  51.9 0.5 multiply_reduce_fusion.1
  52.4 1.6 dynamic-slice_reduce_fusion.2
  54.0 0.6 fusion.61
  54.6 0.1 broadcast_compare_fusion
  54.7 1.9 fusion.11
  56.5 34.6 %all-gather.11.cloned.1.call-done = bf16[32,1024,64]{1,2,0:T(8,128)(2,1)} async-done(((bf16[8,1024,64]{1,2,0:T(8,128)(2,1)}), bf16[32,1024,64]{1,2,0:T(8,128)(2,1)}) %all-gather.11.cloned.1.call-update) | async-done | bytes 4194320 | tf_op jit(solution)/shard_map/all_gather | solution.py:56
  91.1 4.9 copy.56
  96.0 143.2 %all-gather.7.cloned.1.call-done = bf16[2048,2048]{1,0:T(8,128)(2,1)} async-done(((bf16[64,2048]{1,0:T(8,128)(2,1)}), bf16[2048,2048]{1,0:T(8,128)(2,1)}) %all-gather.7.cloned.1.call-update) | async-done | bytes 8388624 | tf_op jit(solution)/shard_map/all_gather | solution.py:37
  239.2 5.1 fusion.37
  244.3 1.0 fusion.52
  245.3 24.3 %all_to_all.26 = f32[2,1,1024]{2,1,0:T(1,128)S(1)} all-to-all(f32[2,1,1024]{2,1,0:T(1,128)S(1)} %broadcast_in_dim.33), channel_id=1, replica_groups=mesh['rep'=2,'fs_0'=2,'fs_1'=4,'fs_2'=4,'tp'=2] {'tp'}, dimensions={0} | all-to-all | bytes 16384 | tf_op jit(solution)/shard_map/all_to_all | solution.py:25
  269.7 1.0 add_convert_fusion.2
  270.7 2.3 reshape.157
  273.1 2.7 bitcast_add_fusion
  275.8 3.0 copy.60
  278.8 3.5 reshape.158
  282.3 5.4 fusion.34
  287.7 2.7 convolution_convert_fusion
  290.4 5.3 all_to_all.27
  295.8 0.4 convert_reduce_fusion.1
  296.2 0.3 add_convert_fusion.1
  296.6 0.3 broadcast_in_dim.37
  296.8 5.5 all_to_all.28
  302.3 0.5 multiply_reduce_fusion
  302.9 0.2 copy-done.10
  303.0 1.9 fusion.9
  304.9 109.0 %all-gather.13.cloned.1.call-done = bf16[2048,2816]{1,0:T(8,128)(2,1)} async-done(((bf16[64,2816]{1,0:T(8,128)(2,1)}), bf16[2048,2816]{1,0:T(8,128)(2,1)}) %all-gather.13.cloned.1.call-update) | async-done | bytes 11534352 | tf_op jit(solution)/shard_map/all_gather | solution.py:37
  413.9 6.8 %fusion.12 = bf16[512,1408]{1,0:T(8,128)(2,1)S(1)} fusion(bf16[512,2048]{1,0:T(8,128)(2,1)} %fusion.9, bf16[2048,2816]{1,0:T(8,128)(2,1)} %all-gather.13.cloned.1.call-done), kind=kOutput, calls=%fused_computation.27 | convolution fusion | flops 2953510912 | bytes 9306112 | tf_op jit(solution)/shard_map/dot_general | solution.py:144
  420.7 1.7 slice.28
  422.4 1.9 slice.29
  424.3 1.2 copy-done.4
  425.5 4.5 fusion.15
  430.0 144.2 %all-gather.15.cloned.1.call-done = bf16[1408,2048]{0,1:T(8,128)(2,1)} async-done(((bf16[1408,64]{0,1:T(8,128)(2,1)}), bf16[1408,2048]{0,1:T(8,128)(2,1)}) %all-gather.15.cloned.1.call-update) | async-done | bytes 5767184 | tf_op jit(solution)/shard_map/all_gather | solution.py:156
  574.2 9.8 %convolution_convert_fusion.1 = bf16[512,2048]{1,0:T(8,128)(2,1)S(1)} fusion(bf16[1408,2048]{0,1:T(8,128)(2,1)} %all-gather.15.cloned.1.call-done, bf16[512,1408]{1,0:T(8,128)(2,1)} %fusion.15, f32[510,1408]{1,0:T(8,128)} %slice.29, f32[511,1408]{1,0:T(8,128)} %slice.28, f32[1408]{0:T(1024)S(1)} %copy-done.13, f32[1408]{0:T(1024)S(1)} %copy-done.12, ...), kind=kOutput, calls=%fused_computation.29 | convolution fusion | flops 2964652032 | bytes 16516096 | tf_op jit(solution)/shard_map/dot_general | solution.py:159
  584.0 25.1 %all_to_all.29 = bf16[2,256,2048]{2,1,0:T(8,128)(2,1)S(1)} all-to-all(bf16[2,256,2048]{2,1,0:T(8,128)(2,1)S(1)} %bitcast.51), channel_id=1, replica_groups=mesh['rep'=2,'fs_0'=2,'fs_1'=4,'fs_2'=4,'tp'=2] {'tp'}, dimensions={0} | all-to-all | bytes 4194304 | tf_op jit(solution)/shard_map/all_to_all | solution.py:74
  609.1 0.4 convert_reduce_fusion
  609.6 1.3 add_convert_fusion
  (58 shorter events, 0.3 us)
Async XLA Ops:
  6.5 48.0 %copy-start = (f32[32,128]{1,0:T(8,128)S(1)}, f32[32,128]{1,0:T(8,128)}, u32[]{:S(2)}) copy-start(f32[32,128]{1,0:T(8,128)} %param.21) | copy-start | bytes 49156
  6.5 32.5 %copy-start.8 = (bf16[64,1024]{1,0:T(8,128)(2,1)S(1)}, bf16[64,1024]{1,0:T(8,128)(2,1)}, u32[]{:S(2)}) copy-start(bf16[64,1024]{1,0:T(8,128)(2,1)} %param.16) | copy-start | bytes 393220
  6.5 32.5 %copy-start.7 = (bf16[64,1024]{1,0:T(8,128)(2,1)S(1)}, bf16[64,1024]{1,0:T(8,128)(2,1)}, u32[]{:S(2)}) copy-start(bf16[64,1024]{1,0:T(8,128)(2,1)} %param.17) | copy-start | bytes 393220
  6.5 33.3 %copy-start.6 = (bf16[64,1408]{1,0:T(8,128)(2,1)S(1)}, bf16[64,1408]{1,0:T(8,128)(2,1)}, u32[]{:S(2)}) copy-start(bf16[64,1408]{1,0:T(8,128)(2,1)} %param.24) | copy-start | bytes 540676
  6.5 33.3 %copy-start.5 = (bf16[64,1408]{1,0:T(8,128)(2,1)S(1)}, bf16[64,1408]{1,0:T(8,128)(2,1)}, u32[]{:S(2)}) copy-start(bf16[64,1408]{1,0:T(8,128)(2,1)} %param.25) | copy-start | bytes 540676
  6.5 34.7 %copy-start.3 = (bf16[256,2048]{1,0:T(8,128)(2,1)S(1)}, bf16[256,2048]{1,0:T(8,128)(2,1)}, u32[]{:S(2)}) copy-start(bf16[256,2048]{1,0:T(8,128)(2,1)} %param.14) | copy-start | bytes 3145732
  6.6 32.4 %all-gather.9.cloned.1.call-start = ((), (), s32[]{:S(2)}) async-start(), calls=%async_computation.6 | async-start | bytes 1310720 | tf_op jit(solution)/shard_map/all_gather | solution.py:56
  14.1 77.0 %all-gather.11.cloned.1.call-start = ((), (), s32[]{:S(2)}) async-start(), calls=%async_computation.7 | async-start | bytes 5242880 | tf_op jit(solution)/shard_map/all_gather | solution.py:56
  39.0 200.2 %all-gather.7.cloned.1.call-start = ((), (), s32[]{:S(2)}) async-start(), calls=%async_computation.5 | async-start | bytes 8650752 | tf_op jit(solution)/shard_map/all_gather | solution.py:37
  39.8 374.0 %all-gather.13.cloned.1.call-start = ((), (), s32[]{:S(2)}) async-start(), calls=%async_computation.8 | async-start | bytes 11894784 | tf_op jit(solution)/shard_map/all_gather | solution.py:37
  40.7 533.5 %all-gather.15.cloned.1.call-start = ((), (), s32[]{:S(2)}) async-start(), calls=%async_computation.9 | async-start | bytes 5947392 | tf_op jit(solution)/shard_map/all_gather | solution.py:156
  42.9 9.0 %all-to-all-start = ((bf16[2,256,2048]{2,1,0:T(8,128)(2,1)}), bf16[2,256,2048]{2,1,0:T(8,128)(2,1)S(1)}, u32[]{:S(2)}, u32[]{:S(2)}) async-start(bf16[2,256,2048]{2,1,0:T(8,128)(2,1)} %broadcast_in_dim.32), calls=%async_computation | async-start | bytes 4194304 | tf_op jit(solution)/shard_map/all_to_all | solution.py:25
  49.4 5.3 copy-start.9
  96.0 173.8 %dynamic-slice-start = ((f32[2048]{0:T(1024)}, s32[]{:T(128)}), f32[1024]{0:T(1024)S(1)}, s32[]{:S(2)}) async-start(f32[2048]{0:T(1024)} %param.18, s32[]{:T(128)} %select_n.51), calls=%async_computation.10 | async-start | bytes 8704 | tf_op jit(solution)/shard_map/dynamic_slice | solution.py:121
  96.0 173.8 %dynamic-slice-start.1 = ((f32[2048]{0:T(1024)}, s32[]{:T(128)}), f32[1024]{0:T(1024)S(1)}, s32[]{:S(2)}) async-start(f32[2048]{0:T(1024)} %param.19, s32[]{:T(128)} %select_n.51), calls=%async_computation.11 | async-start | bytes 8704 | tf_op jit(solution)/shard_map/dynamic_slice | solution.py:122
  282.3 5.4 copy-start.2
  302.3 0.7 copy-start.10
  413.9 10.4 %slice-start = ((s8[11534336]{0:T(1024)(128)(4,1)}), s8[4194304]{0:T(1024)(128)(4,1)S(1)}, s32[]{:S(2)}) async-start(s8[11534336]{0:T(1024)(128)(4,1)} %bitcast.57), calls=%async_computation.12 | async-start | bytes 8388608
  413.9 10.4 %slice-start.1 = ((s8[11534336]{0:T(1024)(128)(4,1)}), s8[4194304]{0:T(1024)(128)(4,1)S(1)}, s32[]{:S(2)}) async-start(s8[11534336]{0:T(1024)(128)(4,1)} %bitcast.57), calls=%async_computation.13 | async-start | bytes 8388608
  420.7 3.6 slice-start.2
  422.4 3.1 copy-start.4
  425.5 148.7 %copy-start.11 = (f32[1408]{0:T(1024)S(1)}, f32[1408]{0:T(1024)}, u32[]{:S(2)}) copy-start(f32[1408]{0:T(1024)} %get-tuple-element.7) | copy-start | bytes 16900
  425.5 148.7 %copy-start.12 = (f32[1408]{0:T(1024)S(1)}, f32[1408]{0:T(1024)}, u32[]{:S(2)}) copy-start(f32[1408]{0:T(1024)} %get-tuple-element.8) | copy-start | bytes 16900
  425.5 148.7 %copy-start.13 = (f32[1408]{0:T(1024)S(1)}, f32[1408]{0:T(1024)}, u32[]{:S(2)}) copy-start(f32[1408]{0:T(1024)} %get-tuple-element.9) | copy-start | bytes 16900
  425.5 148.7 %copy-start.14 = (pred[512]{0:T(512)(128)(4,1)S(1)}, pred[512]{0:T(512)(128)(4,1)}, u32[]{:S(2)}) copy-start(pred[512]{0:T(512)(128)(4,1)} %get-tuple-element.12) | copy-start | bytes 1540
  425.5 148.7 %copy-start.15 = (pred[512]{0:T(512)(128)(4,1)S(1)}, pred[512]{0:T(512)(128)(4,1)}, u32[]{:S(2)}) copy-start(pred[512]{0:T(512)(128)(4,1)} %get-tuple-element.13) | copy-start | bytes 1540
  609.1 1.8 copy-start.1
Sparse Core Ops, SparseCore 0:
  14.2 24.7 all-gather.8
  40.6 50.3 all-gather.10
  92.7 146.3 all-gather.6
  240.7 173.1 all-gather.12
  415.4 158.7 all-gather.14
where the time goes:
time: 618 us; the launch traced here: 617 us
  waiting for transfers between devices  459 us (74%)
  blocking collectives  67.1 us (11%)
  matrix products  37 us (6%)
  local copies, waits for them, and re-layouts  22.9 us (4%)
  between operations  13.4 us (2%)
  other arithmetic  11.5 us (2%)
  starting transfers between devices  6.7 us (1%)
    all_gather x2, waiting for transfers between devices, side_by_side(): out = lax.all_gather(both, axis, axis=dim, tiled=True)  252 us
    all_gather x1, waiting for transfers between devices, on_device(): down_whole = lax.all_gather(down_proj, FS, axis=1, tiled=True)  144 us
    all_gather x2, waiting for transfers between devices, stacked_from(): pieces = lax.all_gather(pieces, axes[k], axis=0, tiled=True)  59.4 us
    all_to_all x2, blocking collectives, sum_at_owner(): lax.all_to_all(pieces, axis, split_axis=0, concat_axis=0, tiled=True)  30.5 us
    all_to_all x2, blocking collectives, copy_for_each(): lax.all_to_all(jnp.broadcast_to(value[None], (devices, *value.shape)), ax...  29.9 us
  transfers between devices with their start and end apart: 6, of which 6 were waited for; matrix products, arithmetic and copies ran while one was open for 9% of the time, Pallas kernels for 0%

commit v1 on v0

--- a/solution.py
+++ b/solution.py
@@ -107,6 +107,10 @@
     conv_taps,
     down_proj,
 ):
+
+    def scenes_save(u):
+        return jnp.concatenate(jax.lax.all_gather(u, axis_name=FS), 1)
+
     position = lax.axis_index("tp")
     rows = gathered_copies(residual, "tp", 0)
     group_rows = rows.shape[0]
@@ -153,7 +157,7 @@
         shifted = jnp.where((offset >= lag)[:, None], shifted, 0.0)
         conv = conv + taps_here[KCONV - 1 - lag] * shifted
     hidden = (jax.nn.silu(conv) * up).astype(jnp.bfloat16)
-    down_whole = lax.all_gather(down_proj, FS, axis=1, tiled=True)
+    down_whole = scenes_save(down_proj)
     part = hidden
     channel_part = sum_at_owner(
         jnp.dot(part, down_whole, preferred_element_type=jnp.float32).astype(jnp.bfloat16), "tp", 0

time: 618 us -> 629 us (1.018)
  waiting for transfers between devices: 459 us -> 472 us
    all_gather x2, waiting for transfers between devices: 252 us -> 270 us  [side_by_side(): out = lax.all_gather(both, axis, axis=dim, tiled=True)]
  transfers between devices with their start and end apart: 6 -> 6, of which waited for: 6 -> 6; matrix products, arithmetic and copies ran while one was open for 9% -> 8% of each run, Pallas kernels for 0% -> 0%
where the time goes in v1:
time: 629 us
  waiting for transfers between devices  472 us (75%)
  blocking collectives  65.8 us (10%)
  matrix products  32.1 us (5%)
  local copies, waits for them, and re-layouts  28.1 us (4%)
  between operations  13.5 us (2%)
  other arithmetic  11 us (2%)
  starting transfers between devices  6.7 us (1%)
    all_gather x2, waiting for transfers between devices, side_by_side(): out = lax.all_gather(both, axis, axis=dim, tiled=True)  270 us
    all_gather x1, waiting for transfers between devices, scenes_save(): return jnp.concatenate(jax.lax.all_gather(u, axis_name=FS), 1)  138 us
    all_gather x2, waiting for transfers between devices, stacked_from(): pieces = lax.all_gather(pieces, axes[k], axis=0, tiled=True)  60.4 us
    all_to_all x2, blocking collectives, copy_for_each(): lax.all_to_all(jnp.broadcast_to(value[None], (devices, *value.shape)), ax...  29.9 us
    all_to_all x2, blocking collectives, sum_at_owner(): lax.all_to_all(pieces, axis, split_axis=0, concat_axis=0, tiled=True)  29.3 us
  transfers between devices with their start and end apart: 6, of which 6 were waited for; matrix products, arithmetic and copies ran while one was open for 8% of the time, Pallas kernels for 0%

profile of v1, /device:TPU:1, one launch (start us, length us, event | category | flops | bytes accessed | tf_op | source)
XLA Modules:
  0.0 628.8 jit_solution(7844085657244020296)
XLA Ops:
  6.6 6.7 %all-gather = bf16[2048,64]{0,1:T(8,128)(2,1)S(1)} all-gather(bf16[1024,64]{0,1:T(8,128)(2,1)} %param.22), channel_id=2, replica_groups=mesh['rep'=2,'fs_0'=2,'fs_1'=4,'fs_2'=4,'tp'=2] {'fs_0'}, dimensions={0}, use_global_device_ids=true | all-gather | bytes 393216 | tf_op jit(solution)/shard_map/all_gather | solution.py:56
  13.3 0.7 copy.80
  14.1 24.9 %all-gather.10.cloned.1.call-done = bf16[8,1024,64]{1,2,0:T(8,128)(2,1)} async-done(((bf16[2,1024,64]{1,2,0:T(8,128)(2,1)}), bf16[8,1024,64]{1,2,0:T(8,128)(2,1)}) %all-gather.10.cloned.1.call-update) | async-done | bytes 1048592 | tf_op jit(solution)/shard_map/all_gather | solution.py:56
  39.1 0.7 all-gather.16.cloned.1.call-update
  39.8 0.7 pad_maximum_fusion.1
  40.6 0.8 pad_maximum_fusion
  41.4 1.6 broadcast_in_dim.32
  43.0 6.5 %all-to-all-start = ((bf16[2,256,2048]{2,1,0:T(8,128)(2,1)}), bf16[2,256,2048]{2,1,0:T(8,128)(2,1)S(1)}, u32[]{:S(2)}, u32[]{:S(2)}) async-start(bf16[2,256,2048]{2,1,0:T(8,128)(2,1)} %broadcast_in_dim.32), calls=%async_computation | async-start | bytes 4194304 | tf_op jit(solution)/shard_map/all_to_all | solution.py:25
  49.5 2.5 all-to-all-done
  52.0 0.5 multiply_reduce_fusion.1
  52.5 1.0 dynamic-slice_reduce_fusion.2
  53.6 0.1 broadcast_compare_fusion
  53.7 1.9 fusion.11
  55.5 35.5 %all-gather.12.cloned.1.call-done = bf16[32,1024,64]{1,2,0:T(8,128)(2,1)} async-done(((bf16[8,1024,64]{1,2,0:T(8,128)(2,1)}), bf16[32,1024,64]{1,2,0:T(8,128)(2,1)}) %all-gather.12.cloned.1.call-update) | async-done | bytes 4194320 | tf_op jit(solution)/shard_map/all_gather | solution.py:56
  91.1 5.0 copy.61
  96.0 138.0 %all-gather.16.cloned.1.call-done = bf16[45056,64]{0,1:T(8,128)(2,1)} async-done(((bf16[1408,64]{0,1:T(8,128)(2,1)}), bf16[45056,64]{0,1:T(8,128)(2,1)}) %all-gather.16.cloned.1.call-update) | async-done | bytes 5767184 | tf_op jit(solution)/shard_map/all_gather | solution.py:112
  234.1 3.5 copy.74
  237.6 4.5 copy.62
  242.1 159.1 %all-gather.8.cloned.1.call-done = bf16[2048,2048]{1,0:T(8,128)(2,1)} async-done(((bf16[64,2048]{1,0:T(8,128)(2,1)}), bf16[2048,2048]{1,0:T(8,128)(2,1)}) %all-gather.8.cloned.1.call-update) | async-done | bytes 8388624 | tf_op jit(solution)/shard_map/all_gather | solution.py:37
  401.2 5.2 fusion.37
  406.3 1.0 fusion.52
  407.3 24.3 %all_to_all.26 = f32[2,1,1024]{2,1,0:T(1,128)S(1)} all-to-all(f32[2,1,1024]{2,1,0:T(1,128)S(1)} %broadcast_in_dim.33), channel_id=1, replica_groups=mesh['rep'=2,'fs_0'=2,'fs_1'=4,'fs_2'=4,'tp'=2] {'tp'}, dimensions={0} | all-to-all | bytes 16384 | tf_op jit(solution)/shard_map/all_to_all | solution.py:25
  431.8 1.0 add_convert_fusion.2
  432.8 2.3 reshape.166
  435.1 2.7 bitcast_add_fusion
  437.8 3.0 copy.66
  440.8 3.5 reshape.167
  444.3 5.4 fusion.34
  449.7 2.7 convolution_convert_fusion
  452.4 5.4 all_to_all.27
  457.7 0.4 convert_reduce_fusion.1
  458.2 0.3 add_convert_fusion.1
  458.5 0.3 broadcast_in_dim.37
  458.8 5.5 all_to_all.28
  464.3 0.5 multiply_reduce_fusion
  464.8 0.2 copy-done.10
  465.0 2.0 fusion.9
  467.0 110.8 %all-gather.14.cloned.1.call-done = bf16[2048,2816]{1,0:T(8,128)(2,1)} async-done(((bf16[64,2816]{1,0:T(8,128)(2,1)}), bf16[2048,2816]{1,0:T(8,128)(2,1)}) %all-gather.14.cloned.1.call-update) | async-done | bytes 11534352 | tf_op jit(solution)/shard_map/all_gather | solution.py:37
  577.8 6.8 %fusion.12 = bf16[512,1408]{1,0:T(8,128)(2,1)S(1)} fusion(bf16[512,2048]{1,0:T(8,128)(2,1)} %fusion.9, bf16[2048,2816]{1,0:T(8,128)(2,1)} %all-gather.14.cloned.1.call-done), kind=kOutput, calls=%fused_computation.27 | convolution fusion | flops 2953510912 | bytes 9306112 | tf_op jit(solution)/shard_map/dot_general | solution.py:148
  584.6 0.2 slice.28
  584.8 0.2 slice.29
  585.1 1.1 copy-done.4
  586.2 0.9 slice-done.4
  587.1 3.4 fusion.15
  590.6 5.9 convolution_convert_fusion.1
  596.5 23.9 %all_to_all.29 = bf16[2,256,2048]{2,1,0:T(8,128)(2,1)S(1)} all-to-all(bf16[2,256,2048]{2,1,0:T(8,128)(2,1)S(1)} %bitcast.63), channel_id=1, replica_groups=mesh['rep'=2,'fs_0'=2,'fs_1'=4,'fs_2'=4,'tp'=2] {'tp'}, dimensions={0} | all-to-all | bytes 4194304 | tf_op jit(solution)/shard_map/all_to_all | solution.py:74
  620.5 0.4 convert_reduce_fusion
  620.9 1.3 add_convert_fusion
  (55 shorter events, 0.4 us)
Async XLA Ops:
  6.5 47.0 %copy-start = (f32[32,128]{1,0:T(8,128)S(1)}, f32[32,128]{1,0:T(8,128)}, u32[]{:S(2)}) copy-start(f32[32,128]{1,0:T(8,128)} %param.21) | copy-start | bytes 49156
  6.5 33.3 %copy-start.8 = (bf16[64,1024]{1,0:T(8,128)(2,1)S(1)}, bf16[64,1024]{1,0:T(8,128)(2,1)}, u32[]{:S(2)}) copy-start(bf16[64,1024]{1,0:T(8,128)(2,1)} %param.16) | copy-start | bytes 393220
  6.5 33.3 %copy-start.7 = (bf16[64,1024]{1,0:T(8,128)(2,1)S(1)}, bf16[64,1024]{1,0:T(8,128)(2,1)}, u32[]{:S(2)}) copy-start(bf16[64,1024]{1,0:T(8,128)(2,1)} %param.17) | copy-start | bytes 393220
  6.5 34.1 %copy-start.6 = (bf16[64,1408]{1,0:T(8,128)(2,1)S(1)}, bf16[64,1408]{1,0:T(8,128)(2,1)}, u32[]{:S(2)}) copy-start(bf16[64,1408]{1,0:T(8,128)(2,1)} %param.24) | copy-start | bytes 540676
  6.5 34.1 %copy-start.5 = (bf16[64,1408]{1,0:T(8,128)(2,1)S(1)}, bf16[64,1408]{1,0:T(8,128)(2,1)}, u32[]{:S(2)}) copy-start(bf16[64,1408]{1,0:T(8,128)(2,1)} %param.25) | copy-start | bytes 540676
  6.5 34.9 %copy-start.3 = (bf16[256,2048]{1,0:T(8,128)(2,1)S(1)}, bf16[256,2048]{1,0:T(8,128)(2,1)}, u32[]{:S(2)}) copy-start(bf16[256,2048]{1,0:T(8,128)(2,1)} %param.14) | copy-start | bytes 3145732
  6.6 32.4 %all-gather.10.cloned.1.call-start = ((), (), s32[]{:S(2)}) async-start(), calls=%async_computation.6 | async-start | bytes 1310720 | tf_op jit(solution)/shard_map/all_gather | solution.py:56
  14.1 77.0 %all-gather.12.cloned.1.call-start = ((), (), s32[]{:S(2)}) async-start(), calls=%async_computation.7 | async-start | bytes 5242880 | tf_op jit(solution)/shard_map/all_gather | solution.py:56
  39.0 195.0 %all-gather.16.cloned.1.call-start = ((), (), s32[]{:S(2)}) async-start(), calls=%async_computation.9 | async-start | bytes 5947392 | tf_op jit(solution)/shard_map/all_gather | solution.py:112
  39.7 361.4 %all-gather.8.cloned.1.call-start = ((), (), s32[]{:S(2)}) async-start(), calls=%async_computation.5 | async-start | bytes 8650752 | tf_op jit(solution)/shard_map/all_gather | solution.py:37
  40.6 537.2 %all-gather.14.cloned.1.call-start = ((), (), s32[]{:S(2)}) async-start(), calls=%async_computation.8 | async-start | bytes 11894784 | tf_op jit(solution)/shard_map/all_gather | solution.py:37
  43.0 9.0 %all-to-all-start = ((bf16[2,256,2048]{2,1,0:T(8,128)(2,1)}), bf16[2,256,2048]{2,1,0:T(8,128)(2,1)S(1)}, u32[]{:S(2)}, u32[]{:S(2)}) async-start(bf16[2,256,2048]{2,1,0:T(8,128)(2,1)} %broadcast_in_dim.32), calls=%async_computation | async-start | bytes 4194304 | tf_op jit(solution)/shard_map/all_to_all | solution.py:25
  49.5 4.1 copy-start.9
  242.1 189.7 %dynamic-slice-start = ((f32[2048]{0:T(1024)}, s32[]{:T(128)}), f32[1024]{0:T(1024)S(1)}, s32[]{:S(2)}) async-start(f32[2048]{0:T(1024)} %param.18, s32[]{:T(128)} %select_n.51), calls=%async_computation.12 | async-start | bytes 8704 | tf_op jit(solution)/shard_map/dynamic_slice | solution.py:125
  242.1 189.7 %dynamic-slice-start.1 = ((f32[2048]{0:T(1024)}, s32[]{:T(128)}), f32[1024]{0:T(1024)S(1)}, s32[]{:S(2)}) async-start(f32[2048]{0:T(1024)} %param.19, s32[]{:T(128)} %select_n.51), calls=%async_computation.13 | async-start | bytes 8704 | tf_op jit(solution)/shard_map/dynamic_slice | solution.py:126
  444.3 5.4 copy-start.2
  464.3 0.7 copy-start.10
  577.8 7.3 %slice-start.2 = ((s8[11534336]{0:T(1024)(128)(4,1)}), s8[4194304]{0:T(1024)(128)(4,1)S(1)}, s32[]{:S(2)}) async-start(s8[11534336]{0:T(1024)(128)(4,1)} %bitcast.69), calls=%async_computation.14 | async-start | bytes 8388608
  577.8 7.3 %slice-start.3 = ((s8[11534336]{0:T(1024)(128)(4,1)}), s8[4194304]{0:T(1024)(128)(4,1)S(1)}, s32[]{:S(2)}) async-start(s8[11534336]{0:T(1024)(128)(4,1)} %bitcast.69), calls=%async_computation.15 | async-start | bytes 8388608
  584.6 1.6 copy-start.4
  584.6 2.5 slice-start.4
  584.8 5.7 slice-start
  587.1 3.4 slice-start.1
  620.5 1.8 copy-start.1
Sparse Core Ops, SparseCore 0:
  14.2 24.7 all-gather.9
  40.6 50.3 all-gather.11
  92.8 141.2 all-gather.15
  235.6 165.5 all-gather.7
  402.7 175.0 all-gather.13
